TPU v7x, 32 devices: a whole 2x2x4 slice. The times are simulated.
32 devices in a mesh: fs: 8 (over z, y), tp: 4 (over x, core).
Axes of the slice: x: 2, y: 2, z: 4, core: 2. Of those that a mesh axis runs over, the one named last changes fastest.
Arguments:
- hidden_in: bfloat16 [512, 4096], P(None, 'tp'), may hold values from -6 to 6
- up_act: bfloat16 [512, 12288], P('tp', 'fs'), may hold values from -6 to 6
- up_val: bfloat16 [512, 12288], P('tp', 'fs'), may hold values from -6 to 6
- cotangent: bfloat16 [512, 4096], P('tp'), may hold values from -6 to 6
- w_act: bfloat16 [4096, 12288], P('tp', 'fs'), may hold values from -0.09375 to 0.09375
- w_val: bfloat16 [4096, 12288], P('tp', 'fs'), may hold values from -0.09375 to 0.09375
- w_down: bfloat16 [12288, 4096], P('fs', 'tp'), may hold values from -0.0546875 to 0.0546875
- conv_act: bfloat16 [3, 12288], P(None, 'fs'), may hold values from -3 to 3
- conv_val: bfloat16 [3, 12288], P(None, 'fs'), may hold values from -3 to 3
- bias_act: bfloat16 [12288], P('fs'), may hold values from -3 to 3
- bias_val: bfloat16 [12288], P('fs'), may hold values from -3 to 3
Outputs:
- grad_input: bfloat16 [512, 4096], P(('tp', 'fs'))
- grad_w_act: float32 [4096, 12288], P('tp', 'fs')
- grad_w_val: float32 [4096, 12288], P('tp', 'fs')
- grad_w_down: float32 [12288, 4096], P('fs', 'tp')
- grad_conv_act: float32 [3, 12288], P(None, 'fs')
- grad_conv_val: float32 [3, 12288], P(None, 'fs')
- grad_bias_act: float32 [12288], P('fs')
- grad_bias_val: float32 [12288], P('fs')
- rows_act: float32 [4096], P('tp')
- rows_val: float32 [4096], P('tp')
- rows_down: float32 [12288], P('fs')
- conv_rows: float32 [2, 3], replicated
All inputs are finite; a program needn't handle non-finite values.
Results may differ from a plain program's by a relative error of at most 0.0057.
Values may be sent and summed in bfloat16 or wider, within the bound.
A program may use at most 128 MiB of HBM per device.

v0:
```python
import jax
import jax.numpy as jnp
from jax import lax
from jax.sharding import PartitionSpec as P


def passed_along(value, axis, by):
    length = lax.axis_size(axis)
    pairs = [(i, i + by) for i in range(length) if 0 <= i + by < length]
    return lax.ppermute(value, axis, pairs)


def contract_last(left, right):
    return lax.dot_general(
        left, right, (((1,), (1,)), ((), ())), preferred_element_type=jnp.float32
    )


def contract_first(left, right):
    return lax.dot_general(
        left, right, (((0,), (0,)), ((), ())), preferred_element_type=jnp.float32
    )


def conv_ahead(extended, taps, bias, length):
    total = jnp.zeros((length, extended.shape[1]), jnp.float32) + bias.astype(jnp.float32)
    for offset in range(taps.shape[0]):
        total = total + taps[offset].astype(jnp.float32) * extended[offset : offset + length]
    return total


def conv_behind(extended, taps, length):
    reach = taps.shape[0] - 1
    total = jnp.zeros((length, extended.shape[1]), jnp.float32)
    for offset in range(taps.shape[0]):
        total = (
            total
            + taps[offset].astype(jnp.float32) * extended[reach - offset : reach - offset + length]
        )
    return total.astype(jnp.bfloat16)


def tap_grads(grad_pre, extended, tap_count):
    length = grad_pre.shape[0]
    rows = [
        jnp.sum(grad_pre * extended[offset : offset + length], axis=0)
        for offset in range(tap_count)
    ]
    return (jnp.stack(rows, 0), jnp.sum(grad_pre, axis=0))


def per_device(
    hidden_in,
    up_act,
    up_val,
    cotangent,
    w_act,
    w_val,
    w_down,
    conv_act,
    conv_val,
    bias_act,
    bias_val,
):
    local_rows = cotangent.shape[0]
    tap_count = conv_act.shape[0]
    reach = tap_count - 1
    tp_count = lax.axis_size("tp")
    fs_count = lax.axis_size("fs")
    down_whole = lax.all_gather(w_down, "tp", axis=1, tiled=True)
    prev_act, prev_val = passed_along(
        (up_act[local_rows - reach :], up_val[local_rows - reach :]), "tp", 1
    )
    ext_act = jnp.concatenate([prev_act, up_act], 0).astype(jnp.float32)
    ext_val = jnp.concatenate([prev_val, up_val], 0).astype(jnp.float32)
    pre_act = conv_ahead(ext_act, conv_act, bias_act, local_rows)
    pre_val = conv_ahead(ext_val, conv_val, bias_val, local_rows)
    gelu_act, gelu_back = jax.vjp(jax.nn.gelu, pre_act)
    mixed = (gelu_act * pre_val).astype(jnp.bfloat16)
    grad_mixed = contract_last(cotangent, down_whole).astype(jnp.bfloat16)
    grad_mixed = lax.optimization_barrier(grad_mixed).astype(jnp.float32)
    grad_pre_act = gelu_back(grad_mixed * pre_val)[0]
    grad_pre_val = grad_mixed * gelu_act
    next_act, next_val = passed_along((grad_pre_act[:reach], grad_pre_val[:reach]), "tp", -1)
    grad_up_act = conv_behind(jnp.concatenate([grad_pre_act, next_act], 0), conv_act, local_rows)
    grad_up_val = conv_behind(jnp.concatenate([grad_pre_val, next_val], 0), conv_val, local_rows)
    taps_act, sums_act = tap_grads(grad_pre_act, ext_act, tap_count)
    taps_val, sums_val = tap_grads(grad_pre_val, ext_val, tap_count)
    all_up_act, all_up_val, all_mixed = (
        lax.all_gather(grad_up_act, "tp", axis=0, tiled=True),
        lax.all_gather(grad_up_val, "tp", axis=0, tiled=True),
        lax.all_gather(mixed, "tp", axis=0, tiled=True),
    )
    cot_columns = lax.all_to_all(cotangent, "tp", split_axis=1, concat_axis=0, tiled=True)
    grad_w_act = contract_first(hidden_in, all_up_act)
    grad_w_val = contract_first(hidden_in, all_up_val)
    grad_w_down = contract_first(all_mixed, cot_columns)
    shard_rows = local_rows // fs_count
    block_rows = tp_count * shard_rows

    def select_rows(gathered):
        shaped = gathered.reshape(tp_count, fs_count, shard_rows, gathered.shape[1])
        return jnp.transpose(shaped, (1, 0, 2, 3)).reshape(
            lax.axis_size("fs") * block_rows, gathered.shape[1]
        )

    summed = lax.psum_scatter(
        contract_last(select_rows(all_up_act), w_act)
        + contract_last(select_rows(all_up_val), w_val),
        "fs",
        scatter_dimension=0,
        tiled=True,
    ).astype(jnp.bfloat16)
    grad_input = lax.all_to_all(summed, "tp", split_axis=0, concat_axis=1, tiled=True)
    down_squares = jnp.sum(grad_w_down * grad_w_down, axis=1)
    taps_act, taps_val, sums_act, sums_val, rows_down = lax.psum(
        (taps_act, taps_val, sums_act, sums_val, down_squares), "tp"
    )
    tap_squares = jnp.stack(
        [jnp.sum(taps_act * taps_act, axis=1), jnp.sum(taps_val * taps_val, axis=1)], 0
    )
    rows_act, rows_val, conv_rows = lax.psum(
        (
            jnp.sum(grad_w_act * grad_w_act, axis=1),
            jnp.sum(grad_w_val * grad_w_val, axis=1),
            tap_squares,
        ),
        "fs",
    )
    return (
        grad_input,
        grad_w_act,
        grad_w_val,
        grad_w_down,
        taps_act,
        taps_val,
        sums_act,
        sums_val,
        rows_act,
        rows_val,
        rows_down,
        conv_rows,
    )


def solution(mesh):
    return jax.shard_map(
        per_device,
        mesh=mesh,
        in_specs=(
            P(None, "tp"),
            P("tp", "fs"),
            P("tp", "fs"),
            P("tp", None),
            P("tp", "fs"),
            P("tp", "fs"),
            P("fs", "tp"),
            P(None, "fs"),
            P(None, "fs"),
            P("fs"),
            P("fs"),
        ),
        out_specs=(
            P(("tp", "fs"), None),
            P("tp", "fs"),
            P("tp", "fs"),
            P("fs", "tp"),
            P(None, "fs"),
            P(None, "fs"),
            P("fs"),
            P("fs"),
            P("tp"),
            P("tp"),
            P("fs"),
            P(),
        ),
        check_vma=False,
    )
```

profile of v0, /device:TPU:0, one launch (start us, length us, event | category | flops | bytes accessed | tf_op | source)
XLA Modules:
  0.0 296.1 jit_solution(9692622403794457745)
XLA Ops:
  8.4 2.4 collective-permute-start.1
  11.5 4.5 %collective-permute-start = (bf16[2,1536]{1,0:T(2,128)(2,1)S(1)}, bf16[2,1536]{1,0:T(2,128)(2,1)S(1)}, u32[]{:S(2)}, u32[]{:S(2)}) collective-permute-start(bf16[2,1536]{1,0:T(2,128)(2,1)S(1)} %slice.74), channel_id=1, source_target_pairs={{0,1},{1,2},{2,3},{4,5},{5,6},{6,7},{8,9},{9,10},{10,11},{12,13},{... | collective-permute-start | bytes 18440 | tf_op jit(solution)/shard_map/ppermute | solution.py:10
  19.8 2.1 maximum_convert_fusion
  21.9 72.5 %all-gather.5.cloned.1.call-done = bf16[1536,4096]{1,0:T(8,128)(2,1)} async-done(((bf16[1536,1024]{1,0:T(8,128)(2,1)}), bf16[1536,4096]{1,0:T(8,128)(2,1)}) %all-gather.5.cloned.1.call-update) | async-done | bytes 12582928 | tf_op jit(solution)/shard_map/all_gather | solution.py:70
  94.4 9.3 %convolution_convert_fusion = bf16[128,1536]{1,0:T(8,128)(2,1)S(1)} fusion(bf16[128,4096]{1,0:T(8,128)(2,1)} %param.14, bf16[1536,4096]{1,0:T(8,128)(2,1)} %all-gather.5.cloned.1.call-done), kind=kOutput, calls=%fused_computation.5 | convolution fusion | flops 1610809344 | bytes 14024704 | tf_op jit(solution)/shard_map/dot_general | solution.py:14
  107.8 2.1 multiply_reduce_fusion.8
  112.1 3.5 %collective-permute-done.2 = f32[2,1536]{1,0:T(2,128)S(1)} collective-permute-done((f32[2,1536]{1,0:T(2,128)S(1)}, f32[2,1536]{1,0:T(2,128)S(1)}, u32[]{:S(2)}, u32[]{:S(2)}) %collective-permute-start.2) | collective-permute-done | bytes 12320 | tf_op jit(solution)/shard_map/ppermute | solution.py:10
  115.5 3.0 fusion.9
  118.6 2.5 multiply_convert_fusion
  121.2 10.4 %all-gather.9.cloned.1.call-done = bf16[512,1536]{1,0:T(8,128)(2,1)} async-done(((bf16[128,1536]{1,0:T(8,128)(2,1)}), bf16[512,1536]{1,0:T(8,128)(2,1)}) %all-gather.9.cloned.1.call-update) | async-done | bytes 1572880 | tf_op jit(solution)/shard_map/all_gather | solution.py:91
  131.5 2.7 copy.34
  134.2 18.6 %all-gather.7.cloned.1.call-done = bf16[512,1536]{1,0:T(8,128)(2,1)} async-done(((bf16[128,1536]{1,0:T(8,128)(2,1)}), bf16[512,1536]{1,0:T(8,128)(2,1)}) %all-gather.7.cloned.1.call-update) | async-done | bytes 1572880 | tf_op jit(solution)/shard_map/all_gather | solution.py:90
  156.7 3.2 %convolution_add_fusion = f32[512,1024]{1,0:T(8,128)} fusion(f32[512,1024]{1,0:T(8,128)S(1)} %fusion.19, bf16[512,1536]{1,0:T(8,128)(2,1)S(1)} %bitcast.37, bf16[1024,1536]{1,0:T(8,128)(2,1)S(1)} %copy-done.17), kind=kOutput, calls=%fused_computation.6 | convolution fusion | flops 1611137024 | bytes 8912896 | tf_op jit(solution)/shard_map/dot_general | solution.py:14
  161.8 21.8 %all_to_all.38 = bf16[128,4,1024]{0,2,1:T(8,128)(2,1)S(1)} all-to-all(bf16[128,4,1024]{0,2,1:T(8,128)(2,1)S(1)} %bitcast.34), channel_id=1, replica_groups=mesh['fs'=8,'tp'=4] {'tp'}, dimensions={1} | all-to-all | bytes 2097152 | tf_op jit(solution)/shard_map/all_to_all | solution.py:94
  185.4 5.8 %multiply_reduce_fusion.1 = (f32[1024]{0:T(1024)S(1)}, f32[1024,1536]{0,1:T(8,128)}) fusion(bf16[512,1536]{1,0:T(8,128)(2,1)S(1)} %copy-done.7, bf16[512,1024]{1,0:T(8,128)(2,1)} %param.11), kind=kOutput, calls=%fused_computation.1 | convolution fusion | flops 1613757440 | bytes 8916992 | tf_op jit(solution)/shard_map/dot_general | solution.py:20
  191.1 6.7 %copy.39 = f32[1024,1536]{1,0:T(8,128)} copy(f32[1024,1536]{0,1:T(8,128)} %get-tuple-element.80) | data formatting | bytes 12582912
  197.8 6.0 %multiply_reduce_fusion = (f32[1536]{0:T(1024)S(1)}, f32[1536,1024]{0,1:T(8,128)}) fusion(bf16[512,1536]{1,0:T(8,128)(2,1)} %all-gather.11.cloned.1.call-done, bf16[512,1024]{1,0:T(8,128)(2,1)S(1)} %bitcast.39), kind=kOutput, calls=%fused_computation | convolution fusion | flops 1613756928 | bytes 8919040 | tf_op jit(solution)/shard_map/dot_general | solution.py:20
  203.8 6.7 %copy.40 = f32[1536,1024]{1,0:T(8,128)} copy(f32[1536,1024]{0,1:T(8,128)} %get-tuple-element.76) | data formatting | bytes 12582912
  210.5 11.9 %all-reduce.1 = (f32[3,1536]{1,0:T(4,128)S(1)}, f32[3,1536]{1,0:T(4,128)S(1)}, f32[1536]{0:T(1024)}, f32[1536]{0:T(1024)}, f32[1536]{0:T(1024)}) all-reduce(f32[3,1536]{1,0:T(4,128)S(1)} %pad_maximum_fusion.2, f32[3,1536]{1,0:T(4,128)S(1)} %pad_maximum_fusion.3, ...), channel_id=1, replica_groups=mesh['fs'=8,'tp'=4] {'tp'}, use_global_device_ids=true, to_apply=%region_4.0 | all-reduce | flops 13824 | bytes 110592 | tf_op jit(solution)/shard_map/psum | solution.py:116
  222.6 28.7 %reduce-scatter.2.cloned.1.call-done = f32[64,1024]{1,0:T(8,128)} async-done(((f32[512,1024]{1,0:T(8,128)}), f32[64,1024]{1,0:T(8,128)}) %reduce-scatter.2.cloned.1.call-update) | async-done | bytes 262160 | tf_op jit(solution)/shard_map/reduce_scatter | solution.py:107
  252.9 3.3 %all-to-all-start = ((bf16[4,16,1024]{2,1,0:T(8,128)(2,1)}), bf16[4,16,1024]{2,1,0:T(8,128)(2,1)S(1)}, u32[]{:S(2)}, u32[]{:S(2)}) async-start(bf16[4,16,1024]{2,1,0:T(8,128)(2,1)} %bitcast.6), calls=%async_computation.1 | async-start | bytes 262144 | tf_op jit(solution)/shard_map/all_to_all | solution.py:114
  256.3 5.7 %multiply_reduce_fusion.2 = (f32[1024]{0:T(1024)S(1)}, f32[1024,1536]{0,1:T(8,128)}) fusion(bf16[512,1536]{1,0:T(8,128)(2,1)S(1)} %copy-done.6, bf16[512,1024]{1,0:T(8,128)(2,1)} %param.11), kind=kOutput, calls=%fused_computation.2 | convolution fusion | flops 1613757440 | bytes 8916992 | tf_op jit(solution)/shard_map/dot_general | solution.py:20
  262.0 6.7 %copy.38 = f32[1024,1536]{1,0:T(8,128)} copy(f32[1024,1536]{0,1:T(8,128)} %get-tuple-element.78) | data formatting | bytes 12582912
  268.7 20.2 %all-reduce = (f32[1024]{0:T(1024)}, f32[1024]{0:T(1024)}, f32[2,3]{1,0:T(2,128)}) all-reduce(f32[1024]{0:T(1024)S(1)} %get-tuple-element.77, f32[1024]{0:T(1024)S(1)} %get-tuple-element.79, f32[2,3]{1,0:T(2,128)S(1)} %pad_maximum_fusion.4), channel_id=1, replica_groups=mesh['fs'=8,'tp'=4] {'fs'}, use_global_device_ids=true, to_apply=%region_14.0 | all-reduce | flops 2054 | bytes 16432 | tf_op jit(solution)/shard_map/psum | solution.py:122
  (79 shorter events, 21.9 us)
Async XLA Ops:
  7.2 147.1 %copy-start = (bf16[1024,1536]{1,0:T(8,128)(2,1)S(1)}, bf16[1024,1536]{1,0:T(8,128)(2,1)}, u32[]{:S(2)}) copy-start(bf16[1024,1536]{1,0:T(8,128)(2,1)} %param.15) | copy-start | bytes 9437188
  7.2 87.2 %all-gather.5.cloned.1.call-start = ((), (), s32[]{:S(2)}) async-start(), calls=%async_computation.3 | async-start | bytes 15728640 | tf_op jit(solution)/shard_map/all_gather | solution.py:70
  7.9 123.6 %all-gather.9.cloned.1.call-start = ((), (), s32[]{:S(2)}) async-start(), calls=%async_computation.5 | async-start | bytes 1966080 | tf_op jit(solution)/shard_map/all_gather | solution.py:91
  8.4 10.4 %collective-permute-start.1 = (bf16[2,1536]{1,0:T(2,128)(2,1)S(1)}, bf16[2,1536]{1,0:T(2,128)(2,1)S(1)}, u32[]{:S(2)}, u32[]{:S(2)}) collective-permute-start(bf16[2,1536]{1,0:T(2,128)(2,1)S(1)} %slice.80), channel_id=1, source_target_pairs={{0,1},{1,2},{2,3},{4,5},{5,6},{6,7},{8,9},{9,10},{10,11},{12,13},{... | collective-permute-start | bytes 18440 | tf_op jit(solution)/shard_map/ppermute | solution.py:10
  11.5 8.3 %collective-permute-start = (bf16[2,1536]{1,0:T(2,128)(2,1)S(1)}, bf16[2,1536]{1,0:T(2,128)(2,1)S(1)}, u32[]{:S(2)}, u32[]{:S(2)}) collective-permute-start(bf16[2,1536]{1,0:T(2,128)(2,1)S(1)} %slice.74), channel_id=1, source_target_pairs={{0,1},{1,2},{2,3},{4,5},{5,6},{6,7},{8,9},{9,10},{10,11},{12,13},{... | collective-permute-start | bytes 18440 | tf_op jit(solution)/shard_map/ppermute | solution.py:10
  21.9 81.8 %copy-start.11 = (f32[1536]{0:T(1024)S(1)}, f32[1536]{0:T(1024)}, u32[]{:S(2)}) copy-start(f32[1536]{0:T(1024)} %get-tuple-element.61) | copy-start | bytes 18436
  21.9 81.8 %copy-start.12 = (f32[1536]{0:T(1024)S(1)}, f32[1536]{0:T(1024)}, u32[]{:S(2)}) copy-start(f32[1536]{0:T(1024)} %convert_element_type.52) | copy-start | bytes 18436
  94.4 9.3 %copy-start.2 = (f32[130,1536]{1,0:T(8,128)S(1)}, f32[130,1536]{1,0:T(8,128)}, u32[]{:S(2)}) copy-start(f32[130,1536]{1,0:T(8,128)} %maximum_convert_fusion.1) | copy-start | bytes 2396164
  94.4 9.3 %copy-start.3 = (f32[130,1536]{1,0:T(8,128)S(1)}, f32[130,1536]{1,0:T(8,128)}, u32[]{:S(2)}) copy-start(f32[130,1536]{1,0:T(8,128)} %maximum_convert_fusion) | copy-start | bytes 2396164
  103.8 2.2 copy-start.13
  103.8 2.3 copy-start.16
  104.7 5.2 %copy-start.4 = (f32[128,1536]{1,0:T(8,128)}, f32[128,1536]{1,0:T(8,128)S(1)}, u32[]{:S(2)}) copy-start(f32[128,1536]{1,0:T(8,128)S(1)} %get-tuple-element.71) | copy-start | bytes 2359300
  104.7 3.1 %collective-permute-start.3 = (f32[2,1536]{1,0:T(2,128)S(1)}, f32[2,1536]{1,0:T(2,128)S(1)}, u32[]{:S(2)}, u32[]{:S(2)}) collective-permute-start(f32[2,1536]{1,0:T(2,128)S(1)} %slice.101), channel_id=1, source_target_pairs={{1,0},{2,1},{3,2},{5,4},{6,5},{7,6},{9,8},{10,9},{11,10},{13,12},{... | collective-permute-start | bytes 36872 | tf_op jit(solution)/shard_map/ppermute | solution.py:10
  109.9 42.9 %all-gather.7.cloned.1.call-start = ((), (), s32[]{:S(2)}) async-start(), calls=%async_computation.4 | async-start | bytes 1966080 | tf_op jit(solution)/shard_map/all_gather | solution.py:90
  110.8 4.8 %collective-permute-start.2 = (f32[2,1536]{1,0:T(2,128)S(1)}, f32[2,1536]{1,0:T(2,128)S(1)}, u32[]{:S(2)}, u32[]{:S(2)}) collective-permute-start(f32[2,1536]{1,0:T(2,128)S(1)} %slice.98), channel_id=1, source_target_pairs={{1,0},{2,1},{3,2},{5,4},{6,5},{7,6},{9,8},{10,9},{11,10},{13,12},{... | collective-permute-start | bytes 36872 | tf_op jit(solution)/shard_map/ppermute | solution.py:10
  118.5 79.3 %all-gather.11.cloned.1.call-start = ((), (), s32[]{:S(2)}) async-start(), calls=%async_computation.7 | async-start | bytes 1966080 | tf_op jit(solution)/shard_map/all_gather | solution.py:92
  121.1 130.2 %reduce-scatter.2.cloned.1.call-start = ((), (), s32[]{:S(2)}) async-start(), calls=%async_computation.6 | async-start | bytes 2359296 | tf_op jit(solution)/shard_map/reduce_scatter | solution.py:107
  154.3 2.4 copy-start.17
  191.1 6.7 %copy-start.9 = (bf16[4,128,1024]{2,1,0:T(8,128)(2,1)S(1)}, bf16[4,128,1024]{2,1,0:T(8,128)(2,1)}, u32[]{:S(2)}) copy-start(bf16[4,128,1024]{2,1,0:T(8,128)(2,1)} %copy.37) | copy-start | bytes 3145732
  203.8 52.5 %copy-start.6 = (bf16[512,1536]{1,0:T(8,128)(2,1)S(1)}, bf16[512,1536]{1,0:T(8,128)(2,1)}, u32[]{:S(2)}) copy-start(bf16[512,1536]{1,0:T(8,128)(2,1)} %all-gather.7.cloned.1.call-done) | copy-start | bytes 4718596
  222.4 39.5 %copy-start.14 = (f32[3,1536]{1,0:T(4,128)}, f32[3,1536]{1,0:T(4,128)S(1)}, u32[]{:S(2)}) copy-start(f32[3,1536]{1,0:T(4,128)S(1)} %get-tuple-element.65) | copy-start | bytes 55300
  222.4 39.5 %copy-start.15 = (f32[3,1536]{1,0:T(4,128)}, f32[3,1536]{1,0:T(4,128)S(1)}, u32[]{:S(2)}) copy-start(f32[3,1536]{1,0:T(4,128)S(1)} %get-tuple-element.66) | copy-start | bytes 55300
  252.9 35.9 %all-to-all-start = ((bf16[4,16,1024]{2,1,0:T(8,128)(2,1)}), bf16[4,16,1024]{2,1,0:T(8,128)(2,1)S(1)}, u32[]{:S(2)}, u32[]{:S(2)}) async-start(bf16[4,16,1024]{2,1,0:T(8,128)(2,1)} %bitcast.6), calls=%async_computation.1 | async-start | bytes 262144 | tf_op jit(solution)/shard_map/all_to_all | solution.py:114
  262.0 27.5 %copy-start.1 = (bf16[1024,1536]{1,0:T(8,128)(2,1)S(1)}, bf16[1024,1536]{1,0:T(8,128)(2,1)}, u32[]{:S(2)}) copy-start(bf16[1024,1536]{1,0:T(8,128)(2,1)} %param.15) | copy-start | bytes 9437188
  (4 other events, 6.1 us)
Sparse Core Ops, SparseCore 0:
  9.6 84.7 all-gather.4
  110.0 21.4 all-gather.8
  133.1 19.6 all-gather.6
  154.2 24.6 all-gather.10
  182.2 68.9 reduce-scatter.1
where the time goes:
time: 297 us; the launch traced here: 296 us
  waiting for transfers between devices  136 us (46%)
  blocking collectives  53.9 us (18%)
  matrix products  31.7 us (11%)
  local copies, waits for them, and re-layouts  31 us (10%)
  other arithmetic  16.2 us (5%)
  between operations  14.1 us (5%)
  starting transfers between devices  13 us (4%)
    all_gather x1, waiting for transfers between devices, per_device(): down_whole = lax.all_gather(w_down, 'tp', axis=1, tiled=True)  72.5 us
    reduce_scatter x1, waiting for transfers between devices, per_device(): lax.psum_scatter(contract_last(select_rows(all_up_act), w_act) + contract...  28.7 us
    unnamed x40, local copies, waits for them, and re-layouts  23.3 us
    all_to_all x1, blocking collectives, per_device(): lax.all_to_all(cotangent, 'tp', split_axis=1, concat_axis=0, tiled=True)  21.8 us
    psum x1, blocking collectives, per_device(): lax.psum((jnp.sum(grad_w_act * grad_w_act, axis=1), jnp.sum(grad_w_val *...  20.2 us
    all_gather x1, waiting for transfers between devices, per_device(): lax.all_gather(grad_up_act, 'tp', axis=0, tiled=True)  18.6 us
    dot_general x3, matrix products, contract_first(): lax.dot_general(left, right, (((0,), (0,)), ((), ())), preferred_element_...  17.5 us
    dot_general x3, matrix products, contract_last(): lax.dot_general(left, right, (((1,), (1,)), ((), ())), preferred_element_...  14.3 us
  transfers between devices with their start and end apart: 10, of which 6 were waited for; matrix products, arithmetic and copies ran while one was open for 21% of the time, Pallas kernels for 0%

commit v1 on v0

--- a/solution.py
+++ b/solution.py
@@ -67,7 +67,7 @@
     reach = tap_count - 1
     tp_count = lax.axis_size("tp")
     fs_count = lax.axis_size("fs")
-    down_whole = lax.all_gather(w_down, "tp", axis=1, tiled=True)
+    down_whole = jnp.concatenate(lax.all_gather(w_down, "tp"), axis=1)
     prev_act, prev_val = passed_along(
         (up_act[local_rows - reach :], up_val[local_rows - reach :]), "tp", 1
     )

time: 297 us -> 313 us (1.054)
  local copies, waits for them, and re-layouts: 31 us -> 45.2 us
    reshape x0 -> x1, local copies, waits for them, and re-layouts: none -> 16.7 us  [per_device(): down_whole = jnp.concatenate(lax.all_gather(w_down, 'tp'), axis=1)]
    unnamed x40 -> x38, local copies, waits for them, and re-layouts: 23.3 us -> 21.4 us
  transfers between devices with their start and end apart: 10 -> 10, of which waited for: 6 -> 6; matrix products, arithmetic and copies ran while one was open for 21% -> 20% of each run, Pallas kernels for 0% -> 0%
where the time goes in v1:
time: 313 us; the launch traced here: 312 us
  waiting for transfers between devices  138 us (44%)
  blocking collectives  55.5 us (18%)
  local copies, waits for them, and re-layouts  45.2 us (14%)
  matrix products  29.3 us (9%)
  other arithmetic  16.3 us (5%)
  between operations  14.1 us (5%)
  starting transfers between devices  13 us (4%)
    all_gather x1, waiting for transfers between devices, per_device(): down_whole = jnp.concatenate(lax.all_gather(w_down, 'tp'), axis=1)  72.8 us
    reduce_scatter x1, waiting for transfers between devices, per_device(): lax.psum_scatter(contract_last(select_rows(all_up_act), w_act) + contract...  30.7 us
    all_to_all x1, blocking collectives, per_device(): lax.all_to_all(cotangent, 'tp', split_axis=1, concat_axis=0, tiled=True)  23 us
    unnamed x38, local copies, waits for them, and re-layouts  21.4 us
    psum x1, blocking collectives, per_device(): lax.psum((jnp.sum(grad_w_act * grad_w_act, axis=1), jnp.sum(grad_w_val *...  20.1 us
    all_gather x1, waiting for transfers between devices, per_device(): lax.all_gather(grad_up_act, 'tp', axis=0, tiled=True)  18.6 us
    dot_general x3, matrix products, contract_first(): lax.dot_general(left, right, (((0,), (0,)), ((), ())), preferred_element_...  17.5 us
    reshape x1, local copies, waits for them, and re-layouts, per_device(): down_whole = jnp.concatenate(lax.all_gather(w_down, 'tp'), axis=1)  16.7 us
  transfers between devices with their start and end apart: 10, of which 6 were waited for; matrix products, arithmetic and copies ran while one was open for 20% of the time, Pallas kernels for 0%

profile of v1, /device:TPU:0, one launch (start us, length us, event | category | flops | bytes accessed | tf_op | source)
XLA Modules:
  0.0 311.6 jit_solution(2727314219239125867)
XLA Ops:
  8.9 2.4 collective-permute-start
  11.3 4.5 %collective-permute-start.1 = (bf16[2,1536]{1,0:T(2,128)(2,1)S(1)}, bf16[2,1536]{1,0:T(2,128)(2,1)S(1)}, u32[]{:S(2)}, u32[]{:S(2)}) collective-permute-start(bf16[2,1536]{1,0:T(2,128)(2,1)S(1)} %slice.80), channel_id=1, source_target_pairs={{0,1},{1,2},{2,3},{4,5},{5,6},{6,7},{8,9},{9,10},{10,11},{12,13},{... | collective-permute-start | bytes 18440 | tf_op jit(solution)/shard_map/ppermute | solution.py:10
  21.6 72.8 %all-gather.12.cloned.1.call-done = bf16[6144,1024]{1,0:T(8,128)(2,1)} async-done(((bf16[1536,1024]{1,0:T(8,128)(2,1)}), bf16[6144,1024]{1,0:T(8,128)(2,1)}) %all-gather.12.cloned.1.call-update) | async-done | bytes 12582928 | tf_op jit(solution)/shard_map/all_gather | solution.py:70
  94.4 16.7 %copy.33 = bf16[1536,4,1024]{0,2,1:T(8,128)(2,1)} copy(bf16[1536,4,1024]{2,0,1:T(8,128)(2,1)} %bitcast.38) | data formatting | bytes 25165824 | tf_op jit(solution)/shard_map/reshape | solution.py:70
  111.1 6.8 %convolution_convert_fusion = bf16[128,1536]{1,0:T(8,128)(2,1)S(1)} fusion(bf16[128,4096]{1,0:T(8,128)(2,1)} %param.14, bf16[1536,4096]{0,1:T(8,128)(2,1)} %bitcast.37), kind=kOutput, calls=%fused_computation.5 | convolution fusion | flops 1610809344 | bytes 14024704 | tf_op jit(solution)/shard_map/dot_general | solution.py:14
  122.0 2.1 multiply_reduce_fusion.8
  126.2 3.5 %collective-permute-done.2 = f32[2,1536]{1,0:T(2,128)S(1)} collective-permute-done((f32[2,1536]{1,0:T(2,128)S(1)}, f32[2,1536]{1,0:T(2,128)S(1)}, u32[]{:S(2)}, u32[]{:S(2)}) %collective-permute-start.2) | collective-permute-done | bytes 12320 | tf_op jit(solution)/shard_map/ppermute | solution.py:10
  129.7 3.0 fusion.9
  132.8 2.6 multiply_convert_fusion
  135.5 10.3 %all-gather.8.cloned.1.call-done = bf16[512,1536]{1,0:T(8,128)(2,1)} async-done(((bf16[128,1536]{1,0:T(8,128)(2,1)}), bf16[512,1536]{1,0:T(8,128)(2,1)}) %all-gather.8.cloned.1.call-update) | async-done | bytes 1572880 | tf_op jit(solution)/shard_map/all_gather | solution.py:91
  145.7 2.7 copy.35
  148.4 18.6 %all-gather.6.cloned.1.call-done = bf16[512,1536]{1,0:T(8,128)(2,1)} async-done(((bf16[128,1536]{1,0:T(8,128)(2,1)}), bf16[512,1536]{1,0:T(8,128)(2,1)}) %all-gather.6.cloned.1.call-update) | async-done | bytes 1572880 | tf_op jit(solution)/shard_map/all_gather | solution.py:90
  170.9 3.2 %convolution_add_fusion = f32[512,1024]{1,0:T(8,128)} fusion(f32[512,1024]{1,0:T(8,128)S(1)} %fusion.19, bf16[512,1536]{1,0:T(8,128)(2,1)S(1)} %bitcast.43, bf16[1024,1536]{1,0:T(8,128)(2,1)S(1)} %copy-done.16), kind=kOutput, calls=%fused_computation.6 | convolution fusion | flops 1611137024 | bytes 8912896 | tf_op jit(solution)/shard_map/dot_general | solution.py:14
  174.7 23.0 %all_to_all.38 = bf16[128,4,1024]{0,2,1:T(8,128)(2,1)S(1)} all-to-all(bf16[128,4,1024]{0,2,1:T(8,128)(2,1)S(1)} %bitcast.40), channel_id=1, replica_groups=mesh['fs'=8,'tp'=4] {'tp'}, dimensions={1} | all-to-all | bytes 2097152 | tf_op jit(solution)/shard_map/all_to_all | solution.py:94
  198.5 6.0 %multiply_reduce_fusion = (f32[1536]{0:T(1024)S(1)}, f32[1536,1024]{0,1:T(8,128)}) fusion(bf16[512,1536]{1,0:T(8,128)(2,1)} %all-gather.10.cloned.1.call-done, bf16[512,1024]{1,0:T(8,128)(2,1)S(1)} %bitcast.45), kind=kOutput, calls=%fused_computation | convolution fusion | flops 1613756928 | bytes 8919040 | tf_op jit(solution)/shard_map/dot_general | solution.py:20
  204.4 6.7 %copy.41 = f32[1536,1024]{1,0:T(8,128)} copy(f32[1536,1024]{0,1:T(8,128)} %get-tuple-element.76) | data formatting | bytes 12582912
  211.2 5.8 %multiply_reduce_fusion.1 = (f32[1024]{0:T(1024)S(1)}, f32[1024,1536]{0,1:T(8,128)}) fusion(bf16[512,1536]{1,0:T(8,128)(2,1)S(1)} %copy-done.7, bf16[512,1024]{1,0:T(8,128)(2,1)} %param.11), kind=kOutput, calls=%fused_computation.1 | convolution fusion | flops 1613757440 | bytes 8916992 | tf_op jit(solution)/shard_map/dot_general | solution.py:20
  216.9 6.7 %copy.40 = f32[1024,1536]{1,0:T(8,128)} copy(f32[1024,1536]{0,1:T(8,128)} %get-tuple-element.80) | data formatting | bytes 12582912
  223.7 12.3 %all-reduce.1 = (f32[3,1536]{1,0:T(4,128)S(1)}, f32[3,1536]{1,0:T(4,128)S(1)}, f32[1536]{0:T(1024)}, f32[1536]{0:T(1024)}, f32[1536]{0:T(1024)}) all-reduce(f32[3,1536]{1,0:T(4,128)S(1)} %pad_maximum_fusion.2, f32[3,1536]{1,0:T(4,128)S(1)} %pad_maximum_fusion.3, ...), channel_id=1, replica_groups=mesh['fs'=8,'tp'=4] {'tp'}, use_global_device_ids=true, to_apply=%region_4.0 | all-reduce | flops 13824 | bytes 110592 | tf_op jit(solution)/shard_map/psum | solution.py:116
  236.1 30.7 %reduce-scatter.2.cloned.1.call-done = f32[64,1024]{1,0:T(8,128)} async-done(((f32[512,1024]{1,0:T(8,128)}), f32[64,1024]{1,0:T(8,128)}) %reduce-scatter.2.cloned.1.call-update) | async-done | bytes 262160 | tf_op jit(solution)/shard_map/reduce_scatter | solution.py:107
  268.5 3.3 %all-to-all-start = ((bf16[4,16,1024]{2,1,0:T(8,128)(2,1)}), bf16[4,16,1024]{2,1,0:T(8,128)(2,1)S(1)}, u32[]{:S(2)}, u32[]{:S(2)}) async-start(bf16[4,16,1024]{2,1,0:T(8,128)(2,1)} %bitcast.9), calls=%async_computation.1 | async-start | bytes 262144 | tf_op jit(solution)/shard_map/all_to_all | solution.py:114
  271.8 5.7 %multiply_reduce_fusion.2 = (f32[1024]{0:T(1024)S(1)}, f32[1024,1536]{0,1:T(8,128)}) fusion(bf16[512,1536]{1,0:T(8,128)(2,1)S(1)} %copy-done.6, bf16[512,1024]{1,0:T(8,128)(2,1)} %param.11), kind=kOutput, calls=%fused_computation.2 | convolution fusion | flops 1613757440 | bytes 8916992 | tf_op jit(solution)/shard_map/dot_general | solution.py:20
  277.5 6.7 %copy.39 = f32[1024,1536]{1,0:T(8,128)} copy(f32[1024,1536]{0,1:T(8,128)} %get-tuple-element.78) | data formatting | bytes 12582912
  284.3 20.1 %all-reduce = (f32[1024]{0:T(1024)}, f32[1024]{0:T(1024)}, f32[2,3]{1,0:T(2,128)}) all-reduce(f32[1024]{0:T(1024)S(1)} %get-tuple-element.77, f32[1024]{0:T(1024)S(1)} %get-tuple-element.79, f32[2,3]{1,0:T(2,128)S(1)} %pad_maximum_fusion.4), channel_id=1, replica_groups=mesh['fs'=8,'tp'=4] {'fs'}, use_global_device_ids=true, to_apply=%region_14.0 | all-reduce | flops 2054 | bytes 16432 | tf_op jit(solution)/shard_map/psum | solution.py:122
  (78 shorter events, 21.3 us)
Async XLA Ops:
  7.2 161.3 %copy-start = (bf16[1024,1536]{1,0:T(8,128)(2,1)S(1)}, bf16[1024,1536]{1,0:T(8,128)(2,1)}, u32[]{:S(2)}) copy-start(bf16[1024,1536]{1,0:T(8,128)(2,1)} %param.15) | copy-start | bytes 9437188
  7.2 4.1 %copy-start.9 = (bf16[128,1536]{1,0:T(8,128)(2,1)S(1)}, bf16[128,1536]{1,0:T(8,128)(2,1)}, u32[]{:S(2)}) copy-start(bf16[128,1536]{1,0:T(8,128)(2,1)} %param.12) | copy-start | bytes 1179652
  7.2 87.2 %all-gather.12.cloned.1.call-start = ((), (), s32[]{:S(2)}) async-start(), calls=%async_computation.7 | async-start | bytes 15728640 | tf_op jit(solution)/shard_map/all_gather | solution.py:70
  7.9 137.8 %all-gather.8.cloned.1.call-start = ((), (), s32[]{:S(2)}) async-start(), calls=%async_computation.4 | async-start | bytes 1966080 | tf_op jit(solution)/shard_map/all_gather | solution.py:91
  8.9 10.7 %collective-permute-start = (bf16[2,1536]{1,0:T(2,128)(2,1)S(1)}, bf16[2,1536]{1,0:T(2,128)(2,1)S(1)}, u32[]{:S(2)}, u32[]{:S(2)}) collective-permute-start(bf16[2,1536]{1,0:T(2,128)(2,1)S(1)} %slice.74), channel_id=1, source_target_pairs={{0,1},{1,2},{2,3},{4,5},{5,6},{6,7},{8,9},{9,10},{10,11},{12,13},{... | collective-permute-start | bytes 18440 | tf_op jit(solution)/shard_map/ppermute | solution.py:10
  11.3 7.3 %collective-permute-start.1 = (bf16[2,1536]{1,0:T(2,128)(2,1)S(1)}, bf16[2,1536]{1,0:T(2,128)(2,1)S(1)}, u32[]{:S(2)}, u32[]{:S(2)}) collective-permute-start(bf16[2,1536]{1,0:T(2,128)(2,1)S(1)} %slice.80), channel_id=1, source_target_pairs={{0,1},{1,2},{2,3},{4,5},{5,6},{6,7},{8,9},{9,10},{10,11},{12,13},{... | collective-permute-start | bytes 18440 | tf_op jit(solution)/shard_map/ppermute | solution.py:10
  111.1 6.8 %copy-start.2 = (f32[130,1536]{1,0:T(8,128)S(1)}, f32[130,1536]{1,0:T(8,128)}, u32[]{:S(2)}) copy-start(f32[130,1536]{1,0:T(8,128)} %maximum_convert_fusion.1) | copy-start | bytes 2396164
  111.1 6.8 %copy-start.3 = (f32[130,1536]{1,0:T(8,128)S(1)}, f32[130,1536]{1,0:T(8,128)}, u32[]{:S(2)}) copy-start(f32[130,1536]{1,0:T(8,128)} %maximum_convert_fusion) | copy-start | bytes 2396164
  111.1 6.9 %copy-start.10 = (f32[1536]{0:T(1024)S(1)}, f32[1536]{0:T(1024)}, u32[]{:S(2)}) copy-start(f32[1536]{0:T(1024)} %get-tuple-element.61) | copy-start | bytes 18436
  111.1 6.9 %copy-start.11 = (f32[1536]{0:T(1024)S(1)}, f32[1536]{0:T(1024)}, u32[]{:S(2)}) copy-start(f32[1536]{0:T(1024)} %convert_element_type.52) | copy-start | bytes 18436
  118.9 5.2 %copy-start.4 = (f32[128,1536]{1,0:T(8,128)}, f32[128,1536]{1,0:T(8,128)S(1)}, u32[]{:S(2)}) copy-start(f32[128,1536]{1,0:T(8,128)S(1)} %get-tuple-element.71) | copy-start | bytes 2359300
  118.9 3.1 collective-permute-start.3
  124.1 42.9 %all-gather.6.cloned.1.call-start = ((), (), s32[]{:S(2)}) async-start(), calls=%async_computation.3 | async-start | bytes 1966080 | tf_op jit(solution)/shard_map/all_gather | solution.py:90
  125.0 4.8 %collective-permute-start.2 = (f32[2,1536]{1,0:T(2,128)S(1)}, f32[2,1536]{1,0:T(2,128)S(1)}, u32[]{:S(2)}, u32[]{:S(2)}) collective-permute-start(f32[2,1536]{1,0:T(2,128)S(1)} %slice.98), channel_id=1, source_target_pairs={{1,0},{2,1},{3,2},{5,4},{6,5},{7,6},{9,8},{10,9},{11,10},{13,12},{... | collective-permute-start | bytes 36872 | tf_op jit(solution)/shard_map/ppermute | solution.py:10
  132.8 65.7 %all-gather.10.cloned.1.call-start = ((), (), s32[]{:S(2)}) async-start(), calls=%async_computation.6 | async-start | bytes 1966080 | tf_op jit(solution)/shard_map/all_gather | solution.py:92
  135.4 131.4 %reduce-scatter.2.cloned.1.call-start = ((), (), s32[]{:S(2)}) async-start(), calls=%async_computation.5 | async-start | bytes 2359296 | tf_op jit(solution)/shard_map/reduce_scatter | solution.py:107
  168.5 2.4 copy-start.16
  170.9 3.2 %copy-start.5 = (bf16[128,4096]{1,0:T(8,128)(2,1)S(1)}, bf16[128,4096]{1,0:T(8,128)(2,1)}, u32[]{:S(2)}) copy-start(bf16[128,4096]{1,0:T(8,128)(2,1)} %param.14) | copy-start | bytes 3145732
  204.4 6.7 %copy-start.7 = (bf16[512,1536]{1,0:T(8,128)(2,1)S(1)}, bf16[512,1536]{1,0:T(8,128)(2,1)}, u32[]{:S(2)}) copy-start(bf16[512,1536]{1,0:T(8,128)(2,1)} %all-gather.8.cloned.1.call-done) | copy-start | bytes 4718596
  216.9 54.9 %copy-start.6 = (bf16[512,1536]{1,0:T(8,128)(2,1)S(1)}, bf16[512,1536]{1,0:T(8,128)(2,1)}, u32[]{:S(2)}) copy-start(bf16[512,1536]{1,0:T(8,128)(2,1)} %all-gather.6.cloned.1.call-done) | copy-start | bytes 4718596
  236.0 41.6 %copy-start.13 = (f32[3,1536]{1,0:T(4,128)}, f32[3,1536]{1,0:T(4,128)S(1)}, u32[]{:S(2)}) copy-start(f32[3,1536]{1,0:T(4,128)S(1)} %get-tuple-element.65) | copy-start | bytes 55300
  236.0 41.6 %copy-start.14 = (f32[3,1536]{1,0:T(4,128)}, f32[3,1536]{1,0:T(4,128)S(1)}, u32[]{:S(2)}) copy-start(f32[3,1536]{1,0:T(4,128)S(1)} %get-tuple-element.66) | copy-start | bytes 55300
  268.5 35.9 %all-to-all-start = ((bf16[4,16,1024]{2,1,0:T(8,128)(2,1)}), bf16[4,16,1024]{2,1,0:T(8,128)(2,1)S(1)}, u32[]{:S(2)}, u32[]{:S(2)}) async-start(bf16[4,16,1024]{2,1,0:T(8,128)(2,1)} %bitcast.9), calls=%async_computation.1 | async-start | bytes 262144 | tf_op jit(solution)/shard_map/all_to_all | solution.py:114
  277.5 27.5 %copy-start.1 = (bf16[1024,1536]{1,0:T(8,128)(2,1)S(1)}, bf16[1024,1536]{1,0:T(8,128)(2,1)}, u32[]{:S(2)}) copy-start(bf16[1024,1536]{1,0:T(8,128)(2,1)} %param.15) | copy-start | bytes 9437188
  (3 other events, 6.4 us)
Sparse Core Ops, SparseCore 0:
  9.6 84.7 all-gather.11
  124.2 21.4 all-gather.7
  147.3 19.6 all-gather.5
  168.4 25.8 all-gather.9
  197.7 69.1 reduce-scatter.1
